TPU v7x, 32 devices: a whole 2x2x4 slice. The times are simulated.
32 devices in a mesh: grp: 2 (over y), ra: 4 (over z), cb: 2 (over x), dp: 2 (over core).
Axes of the slice: x: 2, y: 2, z: 4, core: 2. Of those that a mesh axis runs over, the one named last changes fastest.
Arguments:
- tokens: bfloat16 [256, 2048], P(('grp', 'dp'), 'ra'), parts along dimension 0, may hold values from -62 to 62
- gain_first: float32 [2048], P('ra'), may hold values from 0.1 to 1.9
- up_first: bfloat16 [2048, 8192], P('ra', 'cb'), may hold values from -0.125 to 0.125
- down_first: bfloat16 [8192, 2048], P('cb', 'ra'), may hold values from -0.0625 to 0.0625
- gain_second: float32 [2048], P('ra'), may hold values from 0.1 to 1.9
- up_second: bfloat16 [2048, 8192], P('ra', 'cb'), may hold values from -0.125 to 0.125
- down_second: bfloat16 [8192, 2048], P('cb', 'ra'), may hold values from -0.0625 to 0.0625
- gain_last: float32 [2048], P('ra'), may hold values from 0.1 to 1.9
Outputs:
- normed: bfloat16 [256, 2048], P(('grp', 'dp'), 'ra'), parts along dimension 0
There are 2 independent parts, one for each index of `grp`. A program takes and returns all parts, laid end to end along the dimension named above; an argument that names none is the same for every part. Nothing has to cross between parts.
All inputs are finite; a program needn't handle non-finite values.
Results may differ from a plain program's by a relative error of at most 0.0095.
Values may be sent and summed in bfloat16 or wider, within the bound.
A program may use at most 64 MiB of HBM per device.

v0:
```python
import jax
import jax.numpy as jnp
from jax import lax
from jax.sharding import PartitionSpec as P

D = 2048


EPS = 1e-06


def squares_inverse(h32):
    local_sq = jnp.sum(h32 * h32, axis=1)
    summed_sq = lax.psum(local_sq, "ra")
    return lax.rsqrt(summed_sq / D + EPS)


def activate(summed, inverse):
    return jnp.square(jax.nn.relu(summed * inverse[:, None])).astype(jnp.bfloat16)


def mlp_branch(h32, gain, w_up, w_down):
    scaled = (h32 * gain).astype(jnp.bfloat16)
    partial_value = jnp.dot(scaled, w_up, preferred_element_type=jnp.float32)
    inverse = squares_inverse(h32)
    shared = lax.psum_scatter(partial_value, "ra", scatter_dimension=1, tiled=True)
    hidden_share = activate(shared, inverse)
    down = jnp.dot(
        lax.all_gather(hidden_share, "ra", axis=1, tiled=True),
        w_down,
        preferred_element_type=jnp.float32,
    )
    return lax.psum(down, "cb")


def local(tokens, gain_first, up_first, down_first, gain_second, up_second, down_second, gain_last):
    start32 = tokens.astype(jnp.float32)
    first = (0.5 * start32 + mlp_branch(start32, gain_first, up_first, down_first)).astype(
        jnp.bfloat16
    )
    first32 = first.astype(jnp.float32)
    second = (0.5 * first32 + mlp_branch(first32, gain_second, up_second, down_second)).astype(
        jnp.bfloat16
    )
    second32 = second.astype(jnp.float32)
    inverse = squares_inverse(second32)
    return (second32 * inverse[:, None] * gain_last).astype(jnp.bfloat16)


def solution(mesh):
    return jax.shard_map(
        local,
        mesh=mesh,
        in_specs=(
            P(("grp", "dp"), "ra"),
            P("ra"),
            P("ra", "cb"),
            P("cb", "ra"),
            P("ra"),
            P("ra", "cb"),
            P("cb", "ra"),
            P("ra"),
        ),
        out_specs=P(("grp", "dp"), "ra"),
        check_vma=False,
    )
```

profile of v0, /device:TPU:0, one launch (start us, length us, event | category | flops | bytes accessed | tf_op | source)
XLA Modules:
  0.0 175.9 jit_solution(10254012345547402609)
XLA Ops:
  6.5 0.0 copy-start
  6.5 0.0 reduce-scatter.3.cloned.1.call-start
  6.5 4.1 %fusion.13 = f32[64,4096]{1,0:T(8,128)} fusion(bf16[512,4096]{1,0:T(8,128)(2,1)} %param.10, bf16[64,512]{1,0:T(8,128)(2,1)} %param.8, f32[512]{0:T(512)} %param.9), kind=kOutput, calls=%fused_computation.22 | convolution fusion | flops 268533760 | bytes 5310464 | tf_op jit(solution)/shard_map/dot_general | solution.py:24
  10.6 0.0 copy-start.1
  10.7 0.0 reduce-scatter.3.cloned.1.call-update
  10.7 0.0 all-reduce.3.cloned.1.call-start
  10.7 0.0 copy-done
  10.7 0.1 fusion.6
  10.8 13.5 %psum.35 = f32[64]{0:T(128)S(1)} all-reduce(f32[64]{0:T(128)S(1)} %fusion.6), channel_id=1, replica_groups=mesh['grp'=2,'ra'=4,'cb'=2,'dp'=2] {'ra'}, use_global_device_ids=true, to_apply=%region_2.0 | all-reduce | flops 64 | bytes 512 | tf_op jit(solution)/shard_map/psum | solution.py:14
  24.4 16.5 %reduce-scatter.3.cloned.1.call-done = f32[64,1024]{1,0:T(8,128)} async-done(((f32[64,4096]{1,0:T(8,128)}), f32[64,1024]{1,0:T(8,128)}) %reduce-scatter.3.cloned.1.call-update) | async-done | bytes 262160 | tf_op jit(solution)/shard_map/reduce_scatter | solution.py:26
  40.9 1.0 multiply_convert_fusion.1
  41.9 15.9 %all_gather.6 = bf16[64,4096]{1,0:T(8,128)(2,1)S(1)} all-gather(bf16[64,1024]{1,0:T(8,128)(2,1)S(1)} %multiply_convert_fusion.1), channel_id=1, replica_groups=mesh['grp'=2,'ra'=4,'cb'=2,'dp'=2] {'ra'}, dimensions={1}, use_global_device_ids=true | all-gather | bytes 655360 | tf_op jit(solution)/shard_map/all_gather | solution.py:29
  57.8 3.7 %fusion.18 = f32[64,512]{1,0:T(8,128)} fusion(bf16[64,4096]{1,0:T(8,128)(2,1)S(1)} %all_gather.6, bf16[4096,512]{1,0:T(8,128)(2,1)} %param.11), kind=kOutput, calls=%fused_computation.28 | convolution fusion | flops 268435456 | bytes 4849664 | tf_op jit(solution)/shard_map/dot_general | solution.py:28
  61.5 0.0 all-reduce.3.cloned.1.call-update
  61.5 0.0 reduce-scatter.5.cloned.1.call-start
  61.6 20.1 %all-reduce.3.cloned.1.call-done = f32[64,512]{1,0:T(8,128)} async-done(((f32[64,512]{1,0:T(8,128)}), f32[64,512]{1,0:T(8,128)}) %all-reduce.3.cloned.1.call-update) | async-done | bytes 131088 | tf_op jit(solution)/shard_map/psum | solution.py:33
  81.7 1.0 fusion.10
  82.7 0.0 copy-done.1
  82.7 4.0 %fusion.11 = f32[64,4096]{1,0:T(8,128)} fusion(bf16[512,4096]{1,0:T(8,128)(2,1)} %param.13, bf16[64,512]{1,0:T(8,128)(2,1)S(1)} %get-tuple-element.6, f32[512]{0:T(512)S(1)} %copy-done.1), kind=kOutput, calls=%fused_computation.21 | convolution fusion | flops 268533760 | bytes 5310464 | tf_op jit(solution)/shard_map/dot_general | solution.py:24
  86.7 0.0 reduce-scatter.5.cloned.1.call-update
  86.8 0.0 all-reduce.5.cloned.1.call-start
  86.8 11.9 %psum.37 = f32[64]{0:T(128)S(1)} all-reduce(f32[64]{0:T(128)S(1)} %get-tuple-element.5), channel_id=1, replica_groups=mesh['grp'=2,'ra'=4,'cb'=2,'dp'=2] {'ra'}, use_global_device_ids=true, to_apply=%region_6.7 | all-reduce | flops 64 | bytes 512 | tf_op jit(solution)/shard_map/psum | solution.py:14
  98.7 15.6 %reduce-scatter.5.cloned.1.call-done = f32[64,1024]{1,0:T(8,128)} async-done(((f32[64,4096]{1,0:T(8,128)}), f32[64,1024]{1,0:T(8,128)}) %reduce-scatter.5.cloned.1.call-update) | async-done | bytes 262160 | tf_op jit(solution)/shard_map/reduce_scatter | solution.py:26
  114.3 1.0 multiply_convert_fusion
  115.3 15.9 %all_gather.7 = bf16[64,4096]{1,0:T(8,128)(2,1)S(1)} all-gather(bf16[64,1024]{1,0:T(8,128)(2,1)S(1)} %multiply_convert_fusion), channel_id=1, replica_groups=mesh['grp'=2,'ra'=4,'cb'=2,'dp'=2] {'ra'}, dimensions={1}, use_global_device_ids=true | all-gather | bytes 655360 | tf_op jit(solution)/shard_map/all_gather | solution.py:29
  131.2 3.7 %fusion.19 = f32[64,512]{1,0:T(8,128)} fusion(bf16[64,4096]{1,0:T(8,128)(2,1)S(1)} %all_gather.7, bf16[4096,512]{1,0:T(8,128)(2,1)} %param.14), kind=kOutput, calls=%fused_computation.29 | convolution fusion | flops 268435456 | bytes 4849664 | tf_op jit(solution)/shard_map/dot_general | solution.py:28
  134.9 0.0 all-reduce.5.cloned.1.call-update
  134.9 20.1 %all-reduce.5.cloned.1.call-done = f32[64,512]{1,0:T(8,128)} async-done(((f32[64,512]{1,0:T(8,128)}), f32[64,512]{1,0:T(8,128)}) %all-reduce.5.cloned.1.call-update) | async-done | bytes 131088 | tf_op jit(solution)/shard_map/psum | solution.py:33
  155.0 1.0 fusion
  156.0 11.7 %psum.39 = f32[64]{0:T(128)S(1)} all-reduce(f32[64]{0:T(128)S(1)} %fusion), channel_id=1, replica_groups=mesh['grp'=2,'ra'=4,'cb'=2,'dp'=2] {'ra'}, use_global_device_ids=true, to_apply=%region_9.10 | all-reduce | flops 64 | bytes 512 | tf_op jit(solution)/shard_map/psum | solution.py:14
  167.7 0.0 copy-done.2
  167.7 1.6 fusion.2
  (4 shorter events, 0.0 us)
Async XLA Ops:
  6.5 4.2 %copy-start = (bf16[64,512]{1,0:T(8,128)(2,1)S(1)}, bf16[64,512]{1,0:T(8,128)(2,1)}, u32[]{:S(2)}) copy-start(bf16[64,512]{1,0:T(8,128)(2,1)} %param.8) | copy-start | bytes 196612
  6.5 34.4 %reduce-scatter.3.cloned.1.call-start = ((), (), s32[]{:S(2)}) async-start(), calls=%async_computation.2 | async-start | bytes 1310720 | tf_op jit(solution)/shard_map/reduce_scatter | solution.py:26
  10.6 72.1 %copy-start.1 = (f32[512]{0:T(512)S(1)}, f32[512]{0:T(512)}, u32[]{:S(2)}) copy-start(f32[512]{0:T(512)} %param.12) | copy-start | bytes 6148
  10.7 71.0 %all-reduce.3.cloned.1.call-start = ((), (), s32[]{:S(2)}) async-start(), calls=%async_computation.3 | async-start | bytes 262144 | tf_op jit(solution)/shard_map/psum | solution.py:33
  61.5 52.7 %reduce-scatter.5.cloned.1.call-start = ((), (), s32[]{:S(2)}) async-start(), calls=%async_computation.4 | async-start | bytes 1310720 | tf_op jit(solution)/shard_map/reduce_scatter | solution.py:26
  86.7 81.0 %copy-start.2 = (f32[512]{0:T(512)S(1)}, f32[512]{0:T(512)}, u32[]{:S(2)}) copy-start(f32[512]{0:T(512)} %param.15) | copy-start | bytes 6148
  86.8 68.2 %all-reduce.5.cloned.1.call-start = ((), (), s32[]{:S(2)}) async-start(), calls=%async_computation.5 | async-start | bytes 262144 | tf_op jit(solution)/shard_map/psum | solution.py:33
Sparse Core Ops, SparseCore 0:
  10.8 30.0 reduce-scatter.2
  61.7 19.9 all-reduce.2
  86.9 27.3 reduce-scatter.4
  135.0 19.9 all-reduce.4
where the time goes:
time: 176 us
  waiting for transfers between devices  72.4 us (41%)
  blocking collectives  68.8 us (39%)
  matrix products  15.5 us (9%)
  between operations  13.2 us (8%)
  other arithmetic  5.91 us (3%)
    psum x2, waiting for transfers between devices, mlp_branch(): return lax.psum(down, 'cb')  40.2 us
    psum x3, blocking collectives, squares_inverse(): summed_sq = lax.psum(local_sq, 'ra')  37 us
    reduce_scatter x2, waiting for transfers between devices, mlp_branch(): lax.psum_scatter(partial_value, 'ra', scatter_dimension=1, tiled=True)  32.1 us
    all_gather x2, blocking collectives, mlp_branch(): lax.all_gather(hidden_share, 'ra', axis=1, tiled=True)  31.8 us
    dot_general x2, matrix products, mlp_branch(): partial_value = jnp.dot(scaled, w_up, preferred_element_type=jnp.float32)  8.13 us
    dot_general x2, matrix products, mlp_branch(): jnp.dot(lax.all_gather(hidden_share, 'ra', axis=1, tiled=True), w_down, p...  7.35 us
  transfers between devices with their start and end apart: 4, of which 4 were waited for; matrix products, arithmetic and copies ran while one was open for 0% of the time, Pallas kernels for 0%

commit v1 on v0

v1 whole, which is shorter than its diff:
```python
import functools

import jax
import jax.numpy as jnp
from jax import lax
from jax.experimental import pallas as pl
from jax.experimental.pallas import tpu as pltpu
from jax.sharding import PartitionSpec as P

EPS = 1e-06
MESH = pl.DeviceIdType.MESH
F32, BF16 = jnp.float32, jnp.bfloat16

CHUNK = 512
SPLITS = 2
LAG = 4
SLACK = 4


def kernel(
    n,
    ncb,
    width,
    tokens_ref,
    gain_first,
    up_first,
    down_first,
    gain_second,
    up_second,
    down_second,
    gain_last,
    out_ref,
    up_v,
    down_v,
    h_v,
    scaled_v,
    own_v,
    acc_v,
    branch_v,
    inv_v,
    send_v,
    recv_v,
    sq_send,
    sq_recv,
    cb_send,
    cb_recv,
    up_sem,
    down_sem,
    send_sem,
    recv_sem,
    sq_ssem,
    sq_rsem,
    cb_ssem,
    cb_rsem,
):
    k = lax.axis_index("ra")
    cb = lax.axis_index("cb")
    layers, chunks = up_v.shape[0], up_v.shape[1]
    splits, rows = h_v.shape[0], h_v.shape[1]
    chunk = up_v.shape[3]
    jobs = splits * chunks
    early = jnp.where(2 * k < n, 0, 1)
    late = 1 - early
    early_hops = jnp.where(early == 0, k, n - 1 - k)
    has_early = early_hops > 0
    early_to = jnp.where(early == 0, k + 1, k - 1)
    late_to = jnp.where(early_hops > 0, jnp.where(late == 0, k + 1, k - 1), early_to)
    depth = (n - 1 - 2 * early_hops) * LAG
    gap = max(0, chunks + (n - 1) * LAG + SLACK - jobs)

    def up_copy(layer, c):
        ref = (up_first, up_second)[layer]
        return pltpu.make_async_copy(
            ref.at[:, pl.ds(c * chunk, chunk)], up_v.at[layer, c], up_sem.at[layer, c]
        )

    def down_copy(layer, c):
        ref = (down_first, down_second)[layer]
        return pltpu.make_async_copy(
            ref.at[pl.ds(c * chunk, chunk), :], down_v.at[layer, c], down_sem.at[layer, c]
        )

    for layer in range(layers):
        for c in range(chunks):
            up_copy(layer, c).start()
        for c in range(chunks):
            down_copy(layer, c).start()

    barrier = pltpu.get_barrier_semaphore()
    for off in range(1, n):
        pl.semaphore_signal(
            barrier, inc=1, device_id={"ra": lax.rem(k + off, n)}, device_id_type=MESH
        )
    for off in range(1, ncb):
        pl.semaphore_signal(
            barrier, inc=1, device_id={"cb": lax.rem(cb + off, ncb)}, device_id_type=MESH
        )
    pl.semaphore_wait(barrier, n - 1 + ncb - 1)

    def chain(direction, job, to):
        return pltpu.make_async_remote_copy(
            src_ref=send_v.at[direction, job],
            dst_ref=recv_v.at[direction, job],
            send_sem=send_sem.at[direction, job],
            recv_sem=recv_sem.at[direction, job],
            device_id={"ra": to},
            device_id_type=MESH,
        )

    def sq_copy(level, t, source, off, to):
        return pltpu.make_async_remote_copy(
            src_ref=sq_send.at[level, t],
            dst_ref=sq_recv.at[level, t, source],
            send_sem=sq_ssem.at[level, t, off],
            recv_sem=sq_rsem.at[level, t, source],
            device_id={"ra": to},
            device_id_type=MESH,
        )

    def cb_copy(layer, t, source, off, to):
        return pltpu.make_async_remote_copy(
            src_ref=cb_send.at[layer, t],
            dst_ref=cb_recv.at[layer, t, source],
            send_sem=cb_ssem.at[layer, t, off],
            recv_sem=cb_rsem.at[layer, t, source],
            device_id={"cb": to},
            device_id_type=MESH,
        )

    diagonal = lax.broadcasted_iota(jnp.int32, (rows, 128), 0) == lax.broadcasted_iota(
        jnp.int32, (rows, 128), 1
    )

    def send_squares(level, t, h32):
        total = jnp.sum(h32 * h32, axis=1, keepdims=True)
        line = jnp.sum(jnp.where(diagonal, total, 0.0), axis=0, keepdims=True)
        tile = jnp.broadcast_to(line, (8, 128))
        sq_send[level, t] = tile
        sq_recv[level, t, k] = tile
        for off in range(1, n):
            sq_copy(level, t, k, off, lax.rem(k + off, n)).start()

    def inverse_of(level, t):
        for off in range(1, n):
            source = lax.rem(k + off, n)
            sq_copy(level, t, source, off, source).wait_recv()
        total = sq_recv[level, t, 0]
        for source in range(1, n):
            total = total + sq_recv[level, t, source]
        line = lax.rsqrt(total * (1.0 / width) + EPS)[0:1]
        column = jnp.sum(jnp.where(diagonal, line, 0.0), axis=1, keepdims=True)
        return jnp.broadcast_to(column, (rows, 128))

    def gather_branch(layer, t):
        for off in range(1, ncb):
            source = lax.rem(cb + off, ncb)
            cb_copy(layer, t, source, off, source).wait_recv()
        total = cb_recv[layer, t, 0].astype(F32)
        for source in range(1, ncb):
            total = total + cb_recv[layer, t, source].astype(F32)
        return (0.5 * h_v[t] + total).astype(BF16).astype(F32)

    for t in range(splits):
        h32 = tokens_ref[t * rows : (t + 1) * rows, :].astype(F32)
        h_v[t] = h32
        send_squares(0, t, h32)
        scaled_v[0, t] = (h32 * gain_first[...]).astype(BF16)

    def step(s, _):
        level = jnp.where(
            s < jobs + gap, 0, jnp.where(s < 2 * (jobs + gap), 1, 2)
        )
        at = s - level * (jobs + gap)
        live = at < jobs
        t = jnp.where(live, at // chunks, 0)
        c = at % chunks
        job = level * jobs + at

        @pl.when(live & (c == 0) & (level == 1))
        def _():
            h32 = gather_branch(0, t)
            h_v[t] = h32
            send_squares(1, t, h32)
            scaled_v[1, t] = (h32 * gain_second[...]).astype(BF16)

        @pl.when(live & (c == 0) & (level == 2))
        def _():
            h32 = gather_branch(1, t)
            h_v[t] = h32
            send_squares(2, t, h32)

        for layer in range(layers):

            @pl.when(live & (level == layer) & (t == 0))
            def _():
                up_copy(layer, c).wait()

        @pl.when(live & (level < layers))
        def _():
            own = jnp.dot(scaled_v[level, t], up_v[level, c], preferred_element_type=F32)
            own_v[job] = own

            @pl.when(has_early)
            def _():
                chain(early, job, early_to).wait_recv()
                total = recv_v[early, job].astype(F32) + own
                send_v[early, job] = total.astype(BF16)
                acc_v[job] = total

            @pl.when(jnp.logical_not(has_early))
            def _():
                send_v[early, job] = own.astype(BF16)
                acc_v[job] = own

            chain(early, job, early_to).start()

        s2 = s - depth
        level2 = jnp.where(s2 < jobs + gap, 0, 1)
        at2 = s2 - level2 * (jobs + gap)
        live2 = (s2 >= 0) & (at2 < jobs)
        at2 = jnp.where(live2, at2, 0)
        t2 = at2 // chunks
        c2 = at2 % chunks
        job2 = level2 * jobs + at2

        @pl.when(live2 & (c2 == 0))
        def _():
            inv_v[...] = inverse_of(level2, t2)

        for layer in range(layers):

            @pl.when(live2 & (level2 == layer) & (t2 == 0))
            def _():
                down_copy(layer, c2).wait()

        @pl.when(live2)
        def _():
            chain(late, job2, late_to).wait_recv()
            arrived = recv_v[late, job2].astype(F32)

            @pl.when(has_early)
            def _():
                send_v[late, job2] = (arrived + own_v[job2]).astype(BF16)
                chain(late, job2, late_to).start()

            pre = (arrived + acc_v[job2]) * inv_v[:, 0:1]
            hidden = jnp.square(jnp.maximum(pre, 0.0)).astype(BF16)
            part = jnp.dot(hidden, down_v[level2, c2], preferred_element_type=F32)

            @pl.when(c2 == 0)
            def _():
                branch_v[...] = part

            @pl.when(c2 > 0)
            def _():
                branch_v[...] += part

        @pl.when(live2 & (c2 == chunks - 1))
        def _():
            value = branch_v[...].astype(BF16)
            cb_send[level2, t2] = value
            cb_recv[level2, t2, cb] = value
            for off in range(1, ncb):
                cb_copy(level2, t2, cb, off, lax.rem(cb + off, ncb)).start()

        return 0

    lax.fori_loop(0, 2 * (jobs + gap) + (splits - 1) * chunks + 1, step, 0)

    for t in range(splits):
        inv = inverse_of(2, t)[:, 0:1]
        out_ref[t * rows : (t + 1) * rows, :] = (h_v[t] * inv * gain_last[...]).astype(BF16)

    def drain(job, _):
        chain(early, job, early_to).wait_send()

        @pl.when(has_early)
        def _():
            chain(late, job, late_to).wait_send()

        return 0

    lax.fori_loop(0, layers * jobs, drain, 0)
    for t in range(splits):
        for level in range(layers + 1):
            for off in range(1, n):
                sq_copy(level, t, k, off, lax.rem(k + off, n)).wait_send()
        for layer in range(layers):
            for off in range(1, ncb):
                cb_copy(layer, t, cb, off, lax.rem(cb + off, ncb)).wait_send()


def local(n, ncb, *args):
    tokens, gain_first, up_first, down_first, gain_second, up_second, down_second, gain_last = args
    rows, cols = tokens.shape
    hidden = up_first.shape[1]
    chunk = min(CHUNK, hidden)
    chunks = hidden // chunk
    splits = SPLITS if rows % (16 * SPLITS) == 0 else 1
    part = rows // splits
    jobs = 2 * splits * chunks
    vmem = pl.BlockSpec(memory_space=pltpu.VMEM)
    hbm = pl.BlockSpec(memory_space=pl.ANY)
    dma = pltpu.SemaphoreType.DMA
    return pl.pallas_call(
        functools.partial(kernel, n, ncb, cols * n),
        out_shape=jax.ShapeDtypeStruct((rows, cols), BF16),
        in_specs=[vmem, vmem, hbm, hbm, vmem, hbm, hbm, vmem],
        out_specs=vmem,
        scratch_shapes=[
            pltpu.VMEM((2, chunks, cols, chunk), BF16),
            pltpu.VMEM((2, chunks, chunk, cols), BF16),
            pltpu.VMEM((splits, part, cols), F32),
            pltpu.VMEM((2, splits, part, cols), BF16),
            pltpu.VMEM((jobs, part, chunk), F32),
            pltpu.VMEM((jobs, part, chunk), F32),
            pltpu.VMEM((part, cols), F32),
            pltpu.VMEM((part, 128), F32),
            pltpu.VMEM((2, jobs, part, chunk), BF16),
            pltpu.VMEM((2, jobs, part, chunk), BF16),
            pltpu.VMEM((3, splits, 8, 128), F32),
            pltpu.VMEM((3, splits, n, 8, 128), F32),
            pltpu.VMEM((2, splits, part, cols), BF16),
            pltpu.VMEM((2, splits, ncb, part, cols), BF16),
            dma((2, chunks)),
            dma((2, chunks)),
            dma((2, jobs)),
            dma((2, jobs)),
            dma((3, splits, n)),
            dma((3, splits, n)),
            dma((2, splits, ncb)),
            dma((2, splits, ncb)),
        ],
        compiler_params=pltpu.CompilerParams(
            collective_id=0, has_side_effects=True, vmem_limit_bytes=60 * 1024 * 1024
        ),
    )(
        tokens,
        gain_first.reshape(1, cols),
        up_first,
        down_first,
        gain_second.reshape(1, cols),
        up_second,
        down_second,
        gain_last.reshape(1, cols),
    )


def solution(mesh):
    return jax.shard_map(
        functools.partial(local, mesh.shape["ra"], mesh.shape["cb"]),
        mesh=mesh,
        in_specs=(
            P(("grp", "dp"), "ra"),
            P("ra"),
            P("ra", "cb"),
            P("cb", "ra"),
            P("ra"),
            P("ra", "cb"),
            P("cb", "ra"),
            P("ra"),
        ),
        out_specs=P(("grp", "dp"), "ra"),
        check_vma=False,
    )
```

time: 176 us -> 56.7 us (0.32)
  waiting for transfers between devices: 72.4 us -> 0 us
  blocking collectives: 68.8 us -> 0 us
  Pallas kernels: 0 us -> 55 us
  matrix products: 15.5 us -> 0 us
  between operations: 13.2 us -> 0.01 us
  other arithmetic: 5.91 us -> 0 us
    pallas_call x0 -> x1, Pallas kernels: none -> 55 us  [local(): pl.pallas_call(functools.partial(kernel, n, ncb, cols * n), out_shape=jax...]
    psum x2 -> x0, waiting for transfers between devices: 40.2 us -> none  [mlp_branch(): return lax.psum(down, 'cb')]
    psum x3 -> x0, blocking collectives: 37 us -> none  [squares_inverse(): summed_sq = lax.psum(local_sq, 'ra')]
    reduce_scatter x2 -> x0, waiting for transfers between devices: 32.1 us -> none  [mlp_branch(): lax.psum_scatter(partial_value, 'ra', scatter_dimension=1, tiled=True)]
    all_gather x2 -> x0, blocking collectives: 31.8 us -> none  [mlp_branch(): lax.all_gather(hidden_share, 'ra', axis=1, tiled=True)]
    dot_general x4 -> x0, matrix products: 15.5 us -> none  [the longest x2 8.13 us: mlp_branch(): partial_value = jnp.dot(scaled, w_up, preferred_element_type=jnp.float32)]
    convert_element_type x3 -> x0, other arithmetic: 3.71 us -> none  [the longest x2 2.09 us: activate(): jnp.square(jax.nn.relu(summed * inverse[:, None])).astype(jnp.bfloat16)]
    reduce_sum x3 -> x0, other arithmetic: 2.17 us -> none  [squares_inverse(): local_sq = jnp.sum(h32 * h32, axis=1)]
  transfers between devices with their start and end apart: 4 -> 0, of which waited for: 4 -> 0; matrix products, arithmetic and copies ran while one was open for 0% -> 0% of each run, Pallas kernels for 0% -> 0%
where the time goes in v1:
time: 56.7 us; the launch traced here: 56.5 us
  Pallas kernels  55 us (97%)
  local copies, waits for them, and re-layouts  1.47 us (3%)
    pallas_call x1, Pallas kernels, local(): pl.pallas_call(functools.partial(kernel, n, ncb, cols * n), out_shape=jax...  55 us
    unnamed x1, local copies, waits for them, and re-layouts  1.47 us

profile of v1, /device:TPU:0, one launch (start us, length us, event | category | flops | bytes accessed | tf_op | source)
XLA Modules:
  0.0 56.5 jit_solution(7202655747397614029)
XLA Ops:
  0.0 55.0 %shard_map.82 = bf16[64,512]{1,0:T(8,128)(2,1)} custom-call(bf16[64,512]{1,0:T(8,128)(2,1)} %tokens_ref.1, f32[1,512]{1,0:T(1,128)} %bitcast.3, bf16[512,4096]{1,0:T(8,128)(2,1)} %up_first.1, bf16[4096,512]{1,0:T(8,128)(2,1)} %down_first.1, f32[1,512]{1,0:T(1,128)} %bitcast.4, bf16[512,4096]{1,0:T(8,128)(2,1)} %up_second.1, bf16[4096,512]{1,0:T(8,128)(2,1)} %down_second.1, ...), custom_call_target="tpu_custom_call" | custom-call | tf_op jit(solution)/shard_map/pallas_call | solution.py:305
  55.0 1.5 %copy.10 = bf16[64,512]{1,0:T(8,128)(2,1)} copy(bf16[64,512]{1,0:T(8,128)(2,1)} %shard_map.82) | data formatting | bytes 131072

commit v2 on v1

v2 whole, which is shorter than its diff:
```python
import functools

import jax
import jax.numpy as jnp
from jax import lax
from jax.experimental import pallas as pl
from jax.experimental.pallas import tpu as pltpu
from jax.sharding import PartitionSpec as P

EPS = 1e-06
MESH = pl.DeviceIdType.MESH
F32, BF16 = jnp.float32, jnp.bfloat16

CHUNK = 1024
SPLITS = 4
LAG = 5
SLACK = 4


def kernel(
    n,
    ncb,
    width,
    tokens_ref,
    gain_first,
    up_first,
    down_first,
    gain_second,
    up_second,
    down_second,
    gain_last,
    out_ref,
    tokens_v,
    gain_v,
    out_v,
    up_v,
    down_v,
    h_v,
    scaled_v,
    own_v,
    acc_v,
    branch_v,
    inv_v,
    send_v,
    recv_v,
    sq_send,
    sq_recv,
    cb_send,
    cb_recv,
    in_sem,
    out_sem,
    weight_sem,
    send_sem,
    recv_sem,
    sq_ssem,
    sq_rsem,
    cb_ssem,
    cb_rsem,
):
    k = lax.axis_index("ra")
    cb = lax.axis_index("cb")
    layers, hidden = up_v.shape[0], up_v.shape[2]
    splits, rows = h_v.shape[0], h_v.shape[1]
    chunk = send_v.shape[3]
    chunks = hidden // chunk
    jobs = splits * chunks
    early = jnp.where(2 * k < n, 0, 1)
    late = 1 - early
    early_hops = jnp.where(early == 0, k, n - 1 - k)
    has_early = early_hops > 0
    early_to = jnp.where(early == 0, k + 1, k - 1)
    late_to = jnp.where(early_hops > 0, jnp.where(late == 0, k + 1, k - 1), early_to)
    depth = (n - 1 - 2 * early_hops) * LAG
    gap = max(0, chunks + (n - 1) * LAG + SLACK - jobs)

    def up_copy(layer):
        ref = (up_first, up_second)[layer]
        return pltpu.make_async_copy(ref, up_v.at[layer], weight_sem.at[layer])

    def down_copy(layer):
        ref = (down_first, down_second)[layer]
        return pltpu.make_async_copy(ref, down_v.at[layer], weight_sem.at[layers + layer])

    inputs = [pltpu.make_async_copy(tokens_ref, tokens_v, in_sem.at[0])]
    for i, ref in enumerate((gain_first, gain_second, gain_last)):
        inputs.append(pltpu.make_async_copy(ref, gain_v.at[i], in_sem.at[1 + i]))
    for copy in inputs:
        copy.start()
    up_copy(0).start()

    barrier = pltpu.get_barrier_semaphore()
    for off in range(1, n):
        pl.semaphore_signal(
            barrier, inc=1, device_id={"ra": lax.rem(k + off, n)}, device_id_type=MESH
        )
    for off in range(1, ncb):
        pl.semaphore_signal(
            barrier, inc=1, device_id={"cb": lax.rem(cb + off, ncb)}, device_id_type=MESH
        )
    for copy in inputs:
        copy.wait()
    for t in range(splits):
        h32 = tokens_v[t * rows : (t + 1) * rows, :].astype(F32)
        h_v[t] = h32
        scaled_v[0, t] = (h32 * gain_v[0]).astype(BF16)
    pl.semaphore_wait(barrier, n - 1 + ncb - 1)
    down_copy(0).start()
    up_copy(1).start()
    down_copy(1).start()

    def chain(direction, job, to):
        return pltpu.make_async_remote_copy(
            src_ref=send_v.at[direction, job],
            dst_ref=recv_v.at[direction, job],
            send_sem=send_sem.at[direction],
            recv_sem=recv_sem.at[direction, lax.rem(job, jobs)],
            device_id={"ra": to},
            device_id_type=MESH,
        )

    def sq_copy(level, t, source, to):
        return pltpu.make_async_remote_copy(
            src_ref=sq_send.at[level, t],
            dst_ref=sq_recv.at[level, t, source],
            send_sem=sq_ssem,
            recv_sem=sq_rsem.at[level, t],
            device_id={"ra": to},
            device_id_type=MESH,
        )

    def cb_copy(layer, t, source, to):
        return pltpu.make_async_remote_copy(
            src_ref=cb_send.at[layer, t],
            dst_ref=cb_recv.at[layer, t, source],
            send_sem=cb_ssem,
            recv_sem=cb_rsem.at[layer, t],
            device_id={"cb": to},
            device_id_type=MESH,
        )

    def of_all(ref, ssem, rsem, axis, to):
        return pltpu.make_async_remote_copy(
            src_ref=ref,
            dst_ref=ref,
            send_sem=ssem,
            recv_sem=rsem,
            device_id={axis: to},
            device_id_type=MESH,
        )

    diagonal = lax.broadcasted_iota(jnp.int32, (rows, 128), 0) == lax.broadcasted_iota(
        jnp.int32, (rows, 128), 1
    )

    def send_squares(level, t, h32):
        total = jnp.sum(h32 * h32, axis=1, keepdims=True)
        line = jnp.sum(jnp.where(diagonal, total, 0.0), axis=0, keepdims=True)
        sq_send[level, t] = line
        sq_recv[level, t, k] = line
        for off in range(1, n):
            sq_copy(level, t, k, lax.rem(k + off, n)).start()

    def inverse_of(level, t):
        peers = sq_recv.at[level, t, pl.ds(0, n - 1)]
        of_all(peers, sq_ssem, sq_rsem.at[level, t], "ra", lax.rem(k + 1, n)).wait_recv()
        total = sq_recv[level, t, 0]
        for source in range(1, n):
            total = total + sq_recv[level, t, source]
        line = lax.rsqrt(total * (1.0 / width) + EPS)
        column = jnp.sum(jnp.where(diagonal, line, 0.0), axis=1, keepdims=True)
        return jnp.broadcast_to(column, (rows, 128))

    def gather_branch(layer, t):
        peers = cb_recv.at[layer, t, pl.ds(0, ncb - 1)]
        of_all(peers, cb_ssem, cb_rsem.at[layer, t], "cb", lax.rem(cb + 1, ncb)).wait_recv()
        total = cb_recv[layer, t, 0].astype(F32)
        for source in range(1, ncb):
            total = total + cb_recv[layer, t, source].astype(F32)
        return (0.5 * h_v[t] + total).astype(BF16).astype(F32)

    for t in range(splits):
        send_squares(0, t, h_v[t])

    def step(s, _):
        level = jnp.where(
            s < jobs + gap, 0, jnp.where(s < 2 * (jobs + gap), 1, 2)
        )
        at = s - level * (jobs + gap)
        live = at < jobs
        t = jnp.where(live, at // chunks, 0)
        c = at % chunks
        job = level * jobs + at

        @pl.when(live & (c == 0) & (level == 1))
        def _():
            h32 = gather_branch(0, t)
            h_v[t] = h32
            send_squares(1, t, h32)
            scaled_v[1, t] = (h32 * gain_v[1]).astype(BF16)

        @pl.when(live & (c == 0) & (level == 2))
        def _():
            h32 = gather_branch(1, t)
            h_v[t] = h32
            send_squares(2, t, h32)

        for layer in range(layers):

            @pl.when((level == layer) & (at == 0))
            def _():
                up_copy(layer).wait()

        @pl.when(live & (level < layers))
        def _():
            own = jnp.dot(scaled_v[level, t], up_v[level, :, pl.ds(pl.multiple_of(c * chunk, chunk), chunk)], preferred_element_type=F32)
            own_v[job] = own

            @pl.when(has_early)
            def _():
                chain(early, job, early_to).wait_recv()
                total = recv_v[early, job].astype(F32) + own
                send_v[early, job] = total.astype(BF16)
                acc_v[job] = total

            @pl.when(jnp.logical_not(has_early))
            def _():
                send_v[early, job] = own.astype(BF16)
                acc_v[job] = own

            chain(early, job, early_to).start()

        s2 = s - depth
        level2 = jnp.where(s2 < jobs + gap, 0, 1)
        at2 = s2 - level2 * (jobs + gap)
        live2 = (s2 >= 0) & (at2 < jobs)
        at2 = jnp.where(live2, at2, 0)
        t2 = at2 // chunks
        c2 = at2 % chunks
        job2 = level2 * jobs + at2

        @pl.when(live2 & (c2 == 0))
        def _():
            inv_v[...] = inverse_of(level2, t2)

        for layer in range(layers):

            @pl.when(live2 & (job2 == layer * jobs))
            def _():
                down_copy(layer).wait()

        @pl.when(live2)
        def _():
            chain(late, job2, late_to).wait_recv()
            arrived = recv_v[late, job2].astype(F32)

            @pl.when(has_early)
            def _():
                send_v[late, job2] = (arrived + own_v[job2]).astype(BF16)
                chain(late, job2, late_to).start()

            pre = (arrived + acc_v[job2]) * inv_v[:, 0:1]
            hidden = jnp.square(jnp.maximum(pre, 0.0)).astype(BF16)
            part = jnp.dot(hidden, down_v[level2, pl.ds(pl.multiple_of(c2 * chunk, chunk), chunk), :], preferred_element_type=F32)

            @pl.when(c2 == 0)
            def _():
                branch_v[...] = part

            @pl.when(c2 > 0)
            def _():
                branch_v[...] += part

        @pl.when(live2 & (c2 == chunks - 1))
        def _():
            value = branch_v[...].astype(BF16)
            cb_send[level2, t2] = value
            cb_recv[level2, t2, cb] = value
            for off in range(1, ncb):
                cb_copy(level2, t2, cb, lax.rem(cb + off, ncb)).start()

        return 0

    lax.fori_loop(0, 2 * (jobs + gap) + (splits - 1) * chunks + 1, step, 0)

    def out_copy():
        return pltpu.make_async_copy(out_v, out_ref, out_sem)

    for t in range(splits):
        inv = inverse_of(2, t)[:, 0:1]
        out_v[t * rows : (t + 1) * rows, :] = (h_v[t] * inv * gain_v[2]).astype(BF16)
    out_copy().start()

    of_all(send_v.at[early], send_sem.at[early], recv_sem.at[early, 0], "ra", early_to).wait_send()

    @pl.when(has_early)
    def _():
        of_all(send_v.at[late], send_sem.at[late], recv_sem.at[late, 0], "ra", late_to).wait_send()

    peers = sq_recv.at[:, :, pl.ds(0, n - 1)]
    of_all(peers, sq_ssem, sq_rsem.at[0, 0], "ra", lax.rem(k + 1, n)).wait_send()
    peers = cb_recv.at[:, :, pl.ds(0, ncb - 1)]
    of_all(peers, cb_ssem, cb_rsem.at[0, 0], "cb", lax.rem(cb + 1, ncb)).wait_send()
    out_copy().wait()


def local(n, ncb, *args):
    tokens, gain_first, up_first, down_first, gain_second, up_second, down_second, gain_last = args
    rows, cols = tokens.shape
    hidden = up_first.shape[1]
    chunk = min(CHUNK, hidden)
    chunks = hidden // chunk
    splits = SPLITS if rows % (16 * SPLITS) == 0 else 1
    part = rows // splits
    jobs = 2 * splits * chunks
    hbm = pl.BlockSpec(memory_space=pl.ANY)
    dma = pltpu.SemaphoreType.DMA
    return pl.pallas_call(
        functools.partial(kernel, n, ncb, cols * n),
        out_shape=jax.ShapeDtypeStruct((rows, cols), BF16),
        in_specs=[hbm] * 8,
        out_specs=hbm,
        scratch_shapes=[
            pltpu.VMEM((rows, cols), BF16),
            pltpu.VMEM((3, 1, cols), F32),
            pltpu.VMEM((rows, cols), BF16),
            pltpu.VMEM((2, cols, hidden), BF16),
            pltpu.VMEM((2, hidden, cols), BF16),
            pltpu.VMEM((splits, part, cols), F32),
            pltpu.VMEM((2, splits, part, cols), BF16),
            pltpu.VMEM((jobs, part, chunk), F32),
            pltpu.VMEM((jobs, part, chunk), F32),
            pltpu.VMEM((part, cols), F32),
            pltpu.VMEM((part, 128), F32),
            pltpu.VMEM((2, jobs, part, chunk), BF16),
            pltpu.VMEM((2, jobs, part, chunk), BF16),
            pltpu.VMEM((3, splits, 1, 128), F32),
            pltpu.VMEM((3, splits, n, 1, 128), F32),
            pltpu.VMEM((2, splits, part, cols), BF16),
            pltpu.VMEM((2, splits, ncb, part, cols), BF16),
            dma((4,)),
            dma,
            dma((4,)),
            dma((2,)),
            dma((2, jobs // 2)),
            dma,
            dma((3, splits)),
            dma,
            dma((2, splits)),
        ],
        compiler_params=pltpu.CompilerParams(
            collective_id=0, has_side_effects=True, vmem_limit_bytes=60 * 1024 * 1024
        ),
    )(
        tokens,
        gain_first.reshape(1, cols),
        up_first,
        down_first,
        gain_second.reshape(1, cols),
        up_second,
        down_second,
        gain_last.reshape(1, cols),
    )


def solution(mesh):
    return jax.shard_map(
        functools.partial(local, mesh.shape["ra"], mesh.shape["cb"]),
        mesh=mesh,
        in_specs=(
            P(("grp", "dp"), "ra"),
            P("ra"),
            P("ra", "cb"),
            P("cb", "ra"),
            P("ra"),
            P("ra", "cb"),
            P("cb", "ra"),
            P("ra"),
        ),
        out_specs=P(("grp", "dp"), "ra"),
        check_vma=False,
    )
```

time: 56.7 us -> 50.8 us (0.90)
  Pallas kernels: 55 us -> 49.2 us
    pallas_call x1, Pallas kernels: 55 us -> 49.2 us  [local(): pl.pallas_call(functools.partial(kernel, n, ncb, cols * n), out_shape=jax...]
where the time goes in v2:
time: 50.8 us; the launch traced here: 50.7 us
  Pallas kernels  49.2 us (97%)
  local copies, waits for them, and re-layouts  1.47 us (3%)
    pallas_call x1, Pallas kernels, local(): pl.pallas_call(functools.partial(kernel, n, ncb, cols * n), out_shape=jax...  49.2 us
    unnamed x1, local copies, waits for them, and re-layouts  1.47 us

profile of v2, /device:TPU:0, one launch (start us, length us, event | category | flops | bytes accessed | tf_op | source)
XLA Modules:
  0.0 50.7 jit_solution(1208608237208104408)
XLA Ops:
  0.0 49.2 %shard_map.82 = bf16[64,512]{1,0:T(8,128)(2,1)} custom-call(bf16[64,512]{1,0:T(8,128)(2,1)} %tokens_ref.1, f32[1,512]{1,0:T(1,128)} %bitcast.3, bf16[512,4096]{1,0:T(8,128)(2,1)} %up_first.1, bf16[4096,512]{1,0:T(8,128)(2,1)} %down_first.1, f32[1,512]{1,0:T(1,128)} %bitcast.4, bf16[512,4096]{1,0:T(8,128)(2,1)} %up_second.1, bf16[4096,512]{1,0:T(8,128)(2,1)} %down_second.1, ...), custom_call_target="tpu_custom_call" | custom-call | tf_op jit(solution)/shard_map/pallas_call | solution.py:317
  49.2 1.5 %copy.10 = bf16[64,512]{1,0:T(8,128)(2,1)} copy(bf16[64,512]{1,0:T(8,128)(2,1)} %shard_map.82) | data formatting | bytes 131072

commit v3 on v2

--- a/solution.py
+++ b/solution.py
@@ -14,7 +14,7 @@
 CHUNK = 1024
 SPLITS = 4
 LAG = 5
-SLACK = 4
+SLACK = 3
 
 
 def kernel(
@@ -70,7 +70,7 @@
     has_early = early_hops > 0
     early_to = jnp.where(early == 0, k + 1, k - 1)
     late_to = jnp.where(early_hops > 0, jnp.where(late == 0, k + 1, k - 1), early_to)
-    depth = (n - 1 - 2 * early_hops) * LAG
+    depth = jnp.maximum((n - 1 - 2 * early_hops) * LAG, 1)
     gap = max(0, chunks + (n - 1) * LAG + SLACK - jobs)
 
     def up_copy(layer):
@@ -181,54 +181,16 @@
     for t in range(splits):
         send_squares(0, t, h_v[t])
 
+    def multiply_up(level, t, c):
+        columns = pl.ds(pl.multiple_of(c * chunk, chunk), chunk)
+        own_v[(level * splits + t) * chunks + c] = jnp.dot(
+            scaled_v[level, t], up_v[level, :, columns], preferred_element_type=F32
+        )
+
+    up_copy(0).wait()
+    multiply_up(0, 0, 0)
+
     def step(s, _):
-        level = jnp.where(
-            s < jobs + gap, 0, jnp.where(s < 2 * (jobs + gap), 1, 2)
-        )
-        at = s - level * (jobs + gap)
-        live = at < jobs
-        t = jnp.where(live, at // chunks, 0)
-        c = at % chunks
-        job = level * jobs + at
-
-        @pl.when(live & (c == 0) & (level == 1))
-        def _():
-            h32 = gather_branch(0, t)
-            h_v[t] = h32
-            send_squares(1, t, h32)
-            scaled_v[1, t] = (h32 * gain_v[1]).astype(BF16)
-
-        @pl.when(live & (c == 0) & (level == 2))
-        def _():
-            h32 = gather_branch(1, t)
-            h_v[t] = h32
-            send_squares(2, t, h32)
-
-        for layer in range(layers):
-
-            @pl.when((level == layer) & (at == 0))
-            def _():
-                up_copy(layer).wait()
-
-        @pl.when(live & (level < layers))
-        def _():
-            own = jnp.dot(scaled_v[level, t], up_v[level, :, pl.ds(pl.multiple_of(c * chunk, chunk), chunk)], preferred_element_type=F32)
-            own_v[job] = own
-
-            @pl.when(has_early)
-            def _():
-                chain(early, job, early_to).wait_recv()
-                total = recv_v[early, job].astype(F32) + own
-                send_v[early, job] = total.astype(BF16)
-                acc_v[job] = total
-
-            @pl.when(jnp.logical_not(has_early))
-            def _():
-                send_v[early, job] = own.astype(BF16)
-                acc_v[job] = own
-
-            chain(early, job, early_to).start()
-
         s2 = s - depth
         level2 = jnp.where(s2 < jobs + gap, 0, 1)
         at2 = s2 - level2 * (jobs + gap)
@@ -238,6 +200,15 @@
         c2 = at2 % chunks
         job2 = level2 * jobs + at2
 
+        @pl.when(live2)
+        def _():
+            chain(late, job2, late_to).wait_recv()
+
+            @pl.when(has_early)
+            def _():
+                send_v[late, job2] = (recv_v[late, job2].astype(F32) + own_v[job2]).astype(BF16)
+                chain(late, job2, late_to).start()
+
         @pl.when(live2 & (c2 == 0))
         def _():
             inv_v[...] = inverse_of(level2, t2)
@@ -250,17 +221,10 @@
 
         @pl.when(live2)
         def _():
-            chain(late, job2, late_to).wait_recv()
-            arrived = recv_v[late, job2].astype(F32)
-
-            @pl.when(has_early)
-            def _():
-                send_v[late, job2] = (arrived + own_v[job2]).astype(BF16)
-                chain(late, job2, late_to).start()
-
-            pre = (arrived + acc_v[job2]) * inv_v[:, 0:1]
+            pre = (recv_v[late, job2].astype(F32) + acc_v[job2]) * inv_v[:, 0:1]
             hidden = jnp.square(jnp.maximum(pre, 0.0)).astype(BF16)
-            part = jnp.dot(hidden, down_v[level2, pl.ds(pl.multiple_of(c2 * chunk, chunk), chunk), :], preferred_element_type=F32)
+            rows_at = pl.ds(pl.multiple_of(c2 * chunk, chunk), chunk)
+            part = jnp.dot(hidden, down_v[level2, rows_at, :], preferred_element_type=F32)
 
             @pl.when(c2 == 0)
             def _():
@@ -277,6 +241,59 @@
             cb_recv[level2, t2, cb] = value
             for off in range(1, ncb):
                 cb_copy(level2, t2, cb, lax.rem(cb + off, ncb)).start()
+
+        level = jnp.where(
+            s < jobs + gap, 0, jnp.where(s < 2 * (jobs + gap), 1, 2)
+        )
+        at = s - level * (jobs + gap)
+        live = at < jobs
+        t = jnp.where(live, at // chunks, 0)
+        c = at % chunks
+        job = level * jobs + at
+
+        @pl.when(live & (c == 0) & (level == 1))
+        def _():
+            h32 = gather_branch(0, t)
+            h_v[t] = h32
+            send_squares(1, t, h32)
+            scaled_v[1, t] = (h32 * gain_v[1]).astype(BF16)
+
+            @pl.when(at == 0)
+            def _():
+                up_copy(1).wait()
+
+            multiply_up(1, t, 0)
+
+        @pl.when(live & (c == 0) & (level == 2))
+        def _():
+            h32 = gather_branch(1, t)
+            h_v[t] = h32
+            send_squares(2, t, h32)
+
+        @pl.when(live & (level < layers))
+        def _():
+            own = own_v[job]
+
+            @pl.when(has_early)
+            def _():
+                chain(early, job, early_to).wait_recv()
+                total = recv_v[early, job].astype(F32) + own
+                send_v[early, job] = total.astype(BF16)
+                acc_v[job] = total
+
+            @pl.when(jnp.logical_not(has_early))
+            def _():
+                send_v[early, job] = own.astype(BF16)
+                acc_v[job] = own
+
+            chain(early, job, early_to).start()
+
+        follows = (level < layers) & (at + 1 < jobs)
+        near = jnp.where(follows, at + 1, 0)
+
+        @pl.when(follows & ((level == 0) | (near % chunks > 0)))
+        def _():
+            multiply_up(level, near // chunks, near % chunks)
 
         return 0
 

time: 50.8 us -> 50.7 us (level)
  no operation moved by 1% of the time
where the time goes in v3:
time: 50.7 us; the launch traced here: 50.5 us
  Pallas kernels  49.1 us (97%)
  local copies, waits for them, and re-layouts  1.47 us (3%)
    pallas_call x1, Pallas kernels, local(): pl.pallas_call(functools.partial(kernel, n, ncb, cols * n), out_shape=jax...  49.1 us
    unnamed x1, local copies, waits for them, and re-layouts  1.47 us

profile of v3, /device:TPU:0, one launch (start us, length us, event | category | flops | bytes accessed | tf_op | source)
XLA Modules:
  0.0 50.5 jit_solution(2368067122721515758)
XLA Ops:
  0.0 49.1 %shard_map.82 = bf16[64,512]{1,0:T(8,128)(2,1)} custom-call(bf16[64,512]{1,0:T(8,128)(2,1)} %tokens_ref.1, f32[1,512]{1,0:T(1,128)} %bitcast.3, bf16[512,4096]{1,0:T(8,128)(2,1)} %up_first.1, bf16[4096,512]{1,0:T(8,128)(2,1)} %down_first.1, f32[1,512]{1,0:T(1,128)} %bitcast.4, bf16[512,4096]{1,0:T(8,128)(2,1)} %up_second.1, bf16[4096,512]{1,0:T(8,128)(2,1)} %down_second.1, ...), custom_call_target="tpu_custom_call" | custom-call | tf_op jit(solution)/shard_map/pallas_call | solution.py:334
  49.1 1.5 %copy.10 = bf16[64,512]{1,0:T(8,128)(2,1)} copy(bf16[64,512]{1,0:T(8,128)(2,1)} %shard_map.82) | data formatting | bytes 131072
